TPU v7x, 32 devices: a whole 2x2x4 slice. The times are simulated.
32 devices in a mesh: fs: 4 (over z), rep: 2 (over y), tp: 4 (over x, core).
Axes of the slice: x: 2, y: 2, z: 4, core: 2. Of those that a mesh axis runs over, the one named last changes fastest.
Arguments:
- saved_input: bfloat16 [5120, 3072], P(('fs', 'rep')), may hold values from -6 to 6
- key_cotangent: bfloat16 [5120, 1024], P(('fs', 'rep'), 'tp'), may hold values from -0.0625 to 0.0625
- value_cotangent: bfloat16 [5120, 2048], P(('fs', 'rep'), 'tp'), may hold values from -0.0625 to 0.0625
- key_factor: bfloat16 [3072, 256], replicated, may hold values from -0.375 to 0.375
- value_factor: bfloat16 [3072, 256], replicated, may hold values from -0.375 to 0.375
- key_weight: float32 [3072, 1024], P(('fs', 'rep'), 'tp'), may hold values from -0.109375 to 0.109375
- value_weight: float32 [3072, 2048], P(('fs', 'rep'), 'tp'), may hold values from -0.109375 to 0.109375
- key_first: float32 [256, 1024], P(None, 'tp'), as said below
- key_second: float32 [256, 1024], P(None, 'tp'), may hold values from 0.05 to 1
- value_first: float32 [256, 2048], P(None, 'tp'), as said below
- value_second: float32 [256, 2048], P(None, 'tp'), may hold values from 0.05 to 1
Outputs:
- key_weight_new: float32 [3072, 1024], P(('fs', 'rep'), 'tp')
- value_weight_new: float32 [3072, 2048], P(('fs', 'rep'), 'tp')
- key_first_new: float32 [256, 1024], P(None, 'tp')
- key_second_new: float32 [256, 1024], P(None, 'tp')
- value_first_new: float32 [256, 2048], P(None, 'tp')
- value_second_new: float32 [256, 2048], P(None, 'tp')
- key_step: float32 [3072, 1024], P(('fs', 'rep'), 'tp')
- value_step: float32 [3072, 2048], P(('fs', 'rep'), 'tp')
- key_copy: bfloat16 [3072, 1024], P(None, 'tp')
- value_copy: bfloat16 [3072, 2048], P(None, 'tp')
Inputs may be any that keep to these rules, and one draw needn't show every extreme that they name: `key_first`: real-valued moments whose scale differs from head to head. `value_first`: real-valued moments whose scale differs from head to head.
All inputs are finite; a program needn't handle non-finite values.
Results may differ from a plain program's by a relative error of at most 0.004.
Values may be sent and summed in bfloat16 or wider, within the bound.
A program may use at most 64 MiB of HBM per device.

v0:
```python
import jax
import jax.numpy as jnp
from jax import lax
from jax.sharding import PartitionSpec as P

DK = 1024
DV = 2048
RK = 256
RV = 256


first_decay = 0.8
second_decay = 0.9
epsilon = 1e-08
learn_rate = 0.01


def split_contract(basis, cotangent):
    upper = basis.astype(jnp.bfloat16)
    lower = (basis - upper.astype(jnp.float32)).astype(jnp.bfloat16)
    dims = (((0,), (0,)), ((), ()))
    high_part = lax.dot_general(upper, cotangent, dims, preferred_element_type=jnp.float32)
    low_part = lax.dot_general(lower, cotangent, dims, preferred_element_type=jnp.float32)
    return high_part + low_part


def moments(projection, first, second):
    first_new = first_decay * first + (1.0 - first_decay) * projection
    second_new = second_decay * second + (1.0 - second_decay) * projection * projection
    normed = first_new / (jnp.sqrt(second_new) + epsilon)
    return (first_new, second_new, normed)


def body(
    saved_input,
    key_cotangent,
    value_cotangent,
    key_factor,
    value_factor,
    key_weight,
    value_weight,
    key_first,
    key_second,
    value_first,
    value_second,
):
    local_rows = key_weight.shape[0]
    row_offset = lax.axis_index(("fs", "rep")) * local_rows
    key_rows = lax.dynamic_slice_in_dim(key_factor, row_offset, local_rows, 0).astype(jnp.float32)
    value_rows = lax.dynamic_slice_in_dim(value_factor, row_offset, local_rows, 0).astype(
        jnp.float32
    )
    key_basis = jnp.dot(saved_input, key_factor, preferred_element_type=jnp.float32)
    key_part = split_contract(key_basis, key_cotangent)
    value_basis = jnp.dot(saved_input, value_factor, preferred_element_type=jnp.float32)
    value_part = split_contract(value_basis, value_cotangent)
    key_projected, value_projected = lax.psum((key_part, value_part), ("fs", "rep"))
    key_first_new, key_second_new, key_normed = moments(key_projected, key_first, key_second)
    value_first_new, value_second_new, value_normed = moments(
        value_projected, value_first, value_second
    )
    local_squares = jnp.sum(key_normed * key_normed) + jnp.sum(value_normed * value_normed)
    squares = lax.psum(local_squares, "tp")
    entries = jnp.float32(RK * DK + RV * DV)
    shrink = jnp.sqrt(entries / (entries + squares))
    key_step = shrink * jnp.dot(key_rows, key_normed, precision=lax.Precision.HIGHEST)
    value_step = shrink * jnp.dot(value_rows, value_normed, precision=lax.Precision.HIGHEST)
    key_weight_new = key_weight - learn_rate * key_step
    value_weight_new = value_weight - learn_rate * value_step
    key_copy, value_copy = (
        lax.all_gather(key_weight_new.astype(jnp.bfloat16), ("fs", "rep"), axis=0, tiled=True),
        lax.all_gather(value_weight_new.astype(jnp.bfloat16), ("fs", "rep"), axis=0, tiled=True),
    )
    return (
        key_weight_new,
        value_weight_new,
        key_first_new,
        key_second_new,
        value_first_new,
        value_second_new,
        key_step,
        value_step,
        key_copy,
        value_copy,
    )


def solution(mesh):
    in_specs = (
        P(("fs", "rep"), None),
        P(("fs", "rep"), "tp"),
        P(("fs", "rep"), "tp"),
        P(),
        P(),
        P(("fs", "rep"), "tp"),
        P(("fs", "rep"), "tp"),
        P(None, "tp"),
        P(None, "tp"),
        P(None, "tp"),
        P(None, "tp"),
    )
    out_specs = (
        P(("fs", "rep"), "tp"),
        P(("fs", "rep"), "tp"),
        P(None, "tp"),
        P(None, "tp"),
        P(None, "tp"),
        P(None, "tp"),
        P(("fs", "rep"), "tp"),
        P(("fs", "rep"), "tp"),
        P(None, "tp"),
        P(None, "tp"),
    )
    return jax.shard_map(body, mesh=mesh, in_specs=in_specs, out_specs=out_specs, check_vma=False)
```

profile of v0, /device:TPU:0, one launch (start us, length us, event | category | flops | bytes accessed | tf_op | source)
XLA Modules:
  0.0 225.4 jit_solution(12211310105299718607)
XLA Ops:
  7.2 0.0 copy-start
  7.2 0.0 copy-start.2
  7.2 0.0 all-reduce.3.cloned.1.call-start
  7.2 1.3 copy-done
  8.6 0.0 copy-start.12
  8.6 3.4 %fusion.17 = f32[640,256]{1,0:T(8,128)S(1)} fusion(bf16[640,3072]{1,0:T(8,128)(2,1)} %param.11, bf16[3072,256]{1,0:T(8,128)(2,1)S(1)} %copy-done), kind=kOutput, calls=%fused_computation.31 | convolution fusion | flops 1006632960 | bytes 6160384 | tf_op jit(solution)/shard_map/dot_general | solution.py:55
  12.0 0.0 copy-done.2
  12.1 0.4 fusion.5
  12.5 0.0 copy-start.11
  12.5 1.2 convolution_add_fusion
  13.7 0.0 copy-done.12
  13.7 0.3 copy-done.11
  13.9 0.0 copy-start.5
  13.9 1.2 fusion.16
  15.1 0.0 copy-done.5
  15.1 0.0 copy-start.8
  15.2 0.3 fusion.8
  15.5 1.0 convolution_add_fusion.1
  16.5 0.0 all-reduce.3.cloned.1.call-update
  16.5 0.0 all-gather.3.cloned.1.call-start
  16.6 77.9 %all-reduce.3.cloned.1.call-done = (f32[256,256]{1,0:T(8,128)}, f32[256,512]{1,0:T(8,128)}) async-done(((f32[256,256]{1,0:T(8,128)}, f32[256,512]{1,0:T(8,128)}), (f32[256,256]{1,0:T(8,128)}, f32[256,512]{1,0:T(8,128)})) %all-reduce.3.cloned.1.call-update) | async-done | bytes 786448 | tf_op jit(solution)/shard_map/psum | solution.py:57
  94.5 0.0 copy-start.10
  94.5 0.0 copy-done.8
  94.5 0.0 copy-start.9
  94.5 2.2 multiply_reduce_fusion
  96.7 0.0 copy-start.3
  96.7 0.0 copy-start.4
  96.7 0.0 copy-done.10
  96.7 2.2 multiply_reduce_fusion.1
  98.9 0.0 copy-start.6
  98.9 0.0 copy-start.7
  100.2 6.2 %psum.23 = f32[]{:T(128)} all-reduce(f32[]{:T(128)S(6)} %add.59), channel_id=1, replica_groups=mesh['fs'=4,'rep'=2,'tp'=4] {'tp'}, use_global_device_ids=true, to_apply=%region_4.0 | all-reduce | flops 1 | bytes 8 | tf_op jit(solution)/shard_map/psum | solution.py:63
  107.1 0.0 copy-done.9
  107.1 2.3 %fusion.13 = (bf16[384,256]{1,0:T(8,128)(2,1)}, f32[384,256]{1,0:T(8,128)}, f32[384,256]{1,0:T(8,128)}) fusion(f32[384,256]{1,0:T(8,128)S(1)} %copy-done.9, f32[256,256]{1,0:T(8,128)S(1)} %get-tuple-element.36, f32[256,256]{1,0:T(8,128)S(1)} %get-tuple-element.37, bf16[3072,256]{1,0:T(8,128)(2,1)} %param.14, s32[]{:T(128)S(6)} %select_n.4, f32[]{:T(128)S(6)} %sqrt.11), kind=kOutput, calls=%fused_computation.29 | convolution fusion | flops 302514176 | bytes 2097160 | tf_op jit(solution)/shard_map/dot_general | solution.py:66
  109.4 0.0 all-gather.3.cloned.1.call-update
  109.5 0.0 all-gather.5.cloned.1.call-start
  109.5 0.0 copy-done.3
  109.5 0.0 copy-done.4
  109.5 3.2 %fusion.12 = (bf16[384,512]{1,0:T(8,128)(2,1)}, f32[384,512]{1,0:T(8,128)}, f32[384,512]{1,0:T(8,128)}) fusion(f32[384,512]{1,0:T(8,128)} %param.17, f32[256,512]{1,0:T(8,128)S(1)} %get-tuple-element.38, f32[256,512]{1,0:T(8,128)S(1)} %get-tuple-element.39, bf16[3072,256]{1,0:T(8,128)(2,1)S(1)} %copy-done, s32[]{:T(128)S(6)} %select_n.4, f32[]{:T(128)S(6)} %sqrt.11), kind=kOutput, calls=%fused_computation.28 | convolution fusion | flops 605028352 | bytes 3997704 | tf_op jit(solution)/shard_map/dot_general | solution.py:67
  112.7 0.0 copy-done.6
  112.7 0.0 copy-done.7
  112.7 0.0 all-gather.5.cloned.1.call-update
  112.7 40.5 %all-gather.3.cloned.1.call-done = bf16[3072,256]{1,0:T(8,128)(2,1)} async-done(((bf16[384,256]{1,0:T(8,128)(2,1)}), bf16[3072,256]{1,0:T(8,128)(2,1)}) %all-gather.3.cloned.1.call-update) | async-done | bytes 1572880 | tf_op jit(solution)/shard_map/all_gather | solution.py:71
  153.2 61.2 %all-gather.5.cloned.1.call-done = bf16[3072,512]{1,0:T(8,128)(2,1)} async-done(((bf16[384,512]{1,0:T(8,128)(2,1)}), bf16[3072,512]{1,0:T(8,128)(2,1)}) %all-gather.5.cloned.1.call-update) | async-done | bytes 3145744 | tf_op jit(solution)/shard_map/all_gather | solution.py:72
  214.4 0.0 copy-start.1
  214.4 2.8 %copy.25 = bf16[3072,256]{1,0:T(8,128)(2,1)} copy(bf16[3072,256]{1,0:T(8,128)(2,1)} %all-gather.3.cloned.1.call-done) | data formatting | bytes 3145728
  217.2 0.0 copy-done.1
  217.2 1.7 copy.26
Async XLA Ops:
  7.2 1.4 copy-start
  7.2 4.9 %copy-start.2 = (bf16[640,512]{1,0:T(8,128)(2,1)S(1)}, bf16[640,512]{1,0:T(8,128)(2,1)}, u32[]{:S(2)}) copy-start(bf16[640,512]{1,0:T(8,128)(2,1)} %param.13) | copy-start | bytes 1966084
  7.2 87.3 %all-reduce.3.cloned.1.call-start = ((), (), s32[]{:S(2)}) async-start(), calls=%async_computation.2 | async-start | bytes 1572864 | tf_op jit(solution)/shard_map/psum | solution.py:57
  8.6 5.1 %copy-start.12 = (bf16[640,3072]{1,0:T(8,128)(2,1)S(1)}, bf16[640,3072]{1,0:T(8,128)(2,1)}, u32[]{:S(2)}) copy-start(bf16[640,3072]{1,0:T(8,128)(2,1)} %param.11) | copy-start | bytes 11796484
  12.5 1.5 copy-start.11
  13.9 1.2 copy-start.5
  15.1 79.4 %copy-start.8 = (f32[256,512]{1,0:T(8,128)S(1)}, f32[256,512]{1,0:T(8,128)}, u32[]{:S(2)}) copy-start(f32[256,512]{1,0:T(8,128)} %param.21) | copy-start | bytes 1572868
  16.5 136.7 %all-gather.3.cloned.1.call-start = ((), (), s32[]{:S(2)}) async-start(), calls=%async_computation | async-start | bytes 1769472 | tf_op jit(solution)/shard_map/all_gather | solution.py:71
  94.5 2.2 copy-start.10
  94.5 12.6 %copy-start.9 = (f32[384,256]{1,0:T(8,128)S(1)}, f32[384,256]{1,0:T(8,128)}, u32[]{:S(2)}) copy-start(f32[384,256]{1,0:T(8,128)} %param.16) | copy-start | bytes 1179652
  96.7 12.8 %copy-start.3 = (f32[256,512]{1,0:T(8,128)}, f32[256,512]{1,0:T(8,128)S(1)}, u32[]{:S(2)}) copy-start(f32[256,512]{1,0:T(8,128)S(1)} %get-tuple-element.39) | copy-start | bytes 1572868
  96.7 12.8 %copy-start.4 = (f32[256,512]{1,0:T(8,128)}, f32[256,512]{1,0:T(8,128)S(1)}, u32[]{:S(2)}) copy-start(f32[256,512]{1,0:T(8,128)S(1)} %get-tuple-element.38) | copy-start | bytes 1572868
  98.9 13.8 %copy-start.6 = (f32[256,256]{1,0:T(8,128)}, f32[256,256]{1,0:T(8,128)S(1)}, u32[]{:S(2)}) copy-start(f32[256,256]{1,0:T(8,128)S(1)} %get-tuple-element.37) | copy-start | bytes 786436
  98.9 13.8 %copy-start.7 = (f32[256,256]{1,0:T(8,128)}, f32[256,256]{1,0:T(8,128)S(1)}, u32[]{:S(2)}) copy-start(f32[256,256]{1,0:T(8,128)S(1)} %get-tuple-element.36) | copy-start | bytes 786436
  109.5 104.9 %all-gather.5.cloned.1.call-start = ((), (), s32[]{:S(2)}) async-start(), calls=%async_computation.1 | async-start | bytes 3538944 | tf_op jit(solution)/shard_map/all_gather | solution.py:72
  214.4 2.8 %copy-start.1 = (bf16[3072,512]{1,0:T(8,128)(2,1)S(1)}, bf16[3072,512]{1,0:T(8,128)(2,1)}, u32[]{:S(2)}) copy-start(bf16[3072,512]{1,0:T(8,128)(2,1)} %all-gather.5.cloned.1.call-done) | copy-start | bytes 9437188
Sparse Core Ops, SparseCore 0:
  16.6 77.8 all-reduce.2
  109.6 43.5 all-gather.2
  156.0 58.3 all-gather.4
where the time goes:
time: 226 us; the launch traced here: 225 us
  waiting for transfers between devices  180 us (80%)
  between operations  15.9 us (7%)
  matrix products  13 us (6%)
  blocking collectives  6.17 us (3%)
  local copies, waits for them, and re-layouts  6.12 us (3%)
  other arithmetic  4.39 us (2%)
    psum x1, waiting for transfers between devices, body(): lax.psum((key_part, value_part), ('fs', 'rep'))  77.9 us
    all_gather x1, waiting for transfers between devices, body(): lax.all_gather(value_weight_new.astype(jnp.bfloat16), ('fs', 'rep'), axis...  61.2 us
    all_gather x1, waiting for transfers between devices, body(): lax.all_gather(key_weight_new.astype(jnp.bfloat16), ('fs', 'rep'), axis=0...  40.5 us
    psum x1, blocking collectives, body(): squares = lax.psum(local_squares, 'tp')  6.17 us
    unnamed x28, local copies, waits for them, and re-layouts  6.12 us
  transfers between devices with their start and end apart: 3, of which 3 were waited for; matrix products, arithmetic and copies ran while one was open for 1% of the time, Pallas kernels for 0%

commit v1 on v0

v1 whole, which is shorter than its diff:
```python
import functools
import math

import jax
import jax.numpy as jnp
from jax import lax
from jax.experimental import pallas as pl
from jax.experimental.pallas import tpu as pltpu
from jax.sharding import PartitionSpec as P

first_decay = 0.8
second_decay = 0.9
epsilon = 1e-08
learn_rate = 0.01

SCATTER_TYPE = jnp.float32
GATHER_TYPE = jnp.float32
MESH = pl.DeviceIdType.MESH


def moments(projection, first, second):
    first_new = first_decay * first + (1.0 - first_decay) * projection
    second_new = second_decay * second + (1.0 - second_decay) * projection * projection
    normed = first_new / (jnp.sqrt(second_new) + epsilon)
    return (first_new, second_new, normed)


def contract(basis, cotangent):
    upper = basis.astype(jnp.bfloat16)
    lower = (basis - upper.astype(jnp.float32)).astype(jnp.bfloat16)
    dims = (((0,), (0,)), ((), ()))
    high_part = lax.dot_general(upper, cotangent, dims, preferred_element_type=jnp.float32)
    low_part = lax.dot_general(lower, cotangent, dims, preferred_element_type=jnp.float32)
    return high_part + low_part


class Plan:
    def __init__(self, mesh_shape, rows, rank, key_cols, value_cols):
        self.F, self.R, self.T = (mesh_shape[a] for a in ("fs", "rep", "tp"))
        self.rows, self.rank = rows, rank
        self.kc, self.vc = key_cols, value_cols
        self.cols = key_cols + value_cols
        self.piece = math.gcd(rows, 64)
        self.pieces = rows // self.piece
        self.dup = 1 if self.R == 2 and self.pieces >= 4 else 0
        self.half = self.rank // self.R
        owners = self.F
        while self.half % owners or (self.half // owners) % 16 or self.F % owners:
            owners -= 1
        self.owners = owners
        self.slice = self.half // owners


def kernel(
    plan,
    x_hbm, kcot_hbm, vcot_hbm, kfac_hbm, vfac_hbm, kw, vw, kf, ks, vf, vs,
    wall, kf_out, ks_out, vf_out, vs_out, normed_out, squares_out,
    x, kcot, vcot, kfac, vfac, partial, ysend, yrecv, half, zsend, zrecv, total, sq,
    load_sem, zs_sem, zr_sem, ys_sem, yr_sem, ds_sem, dr_sem,
    rys, ryr, rzs, rzr, gzs, gzr, gys, gyr, ts, tr,
):
    F, R, T = plan.F, plan.R, plan.T
    NP, PR, C = plan.pieces, plan.piece, plan.cols
    z = lax.axis_index("fs")
    y = lax.axis_index("rep")
    t = lax.axis_index("tp")

    loads = [
        pltpu.make_async_copy(s, d, load_sem.at[i])
        for i, (s, d) in enumerate(
            ((x_hbm, x), (kfac_hbm, kfac), (kcot_hbm, kcot), (vfac_hbm, vfac), (vcot_hbm, vcot))
        )
    ]
    for c in loads:
        c.start()

    def fs_peer(j):
        return lax.rem(z + j, F)

    def rep_peer(j):
        return lax.rem(y + j, R)

    def tp_peer(j):
        return lax.rem(t + j, T)

    barrier = pltpu.get_barrier_semaphore()
    for axis, size, peer in (("fs", F, fs_peer), ("rep", R, rep_peer), ("tp", T, tp_peer)):
        for j in range(1, size):
            pl.semaphore_signal(barrier, 1, device_id={axis: peer(j)}, device_id_type=MESH)

    own = wall.at[z, y]
    own[:, : plan.kc] = kw[...].astype(jnp.bfloat16)
    own[:, plan.kc :] = vw[...].astype(jnp.bfloat16)
    pl.semaphore_wait(barrier, F + R + T - 3)

    def rc(src, dst, s, r, axis, target):
        return pltpu.make_async_remote_copy(
            src_ref=src, dst_ref=dst, send_sem=s, recv_sem=r,
            device_id={axis: target}, device_id_type=MESH,
        )

    def prows(p):
        return pl.ds(p * PR, PR)

    def fs_copy(direction, s, p, wait=False):
        if direction == 0:
            source, target, ok = z - s, z + 1, z < F - 1
        else:
            source, target, ok = z + s, z - 1, z > 0
        source = jnp.clip(source, 0, F - 1)
        target = jnp.clip(target, 0, F - 1)
        ref = wall.at[source, y, prows(p)]
        sem = s if wait else s + 1
        return rc(ref, ref, zs_sem.at[direction, s, p], zr_sem.at[direction, sem, p], "fs", target)

    def dup_copy(direction, s, wait=False):
        if direction == 0:
            source, target = z - s, z + 1
        else:
            source, target = z + s, z - 1
        source = jnp.clip(source, 0, F - 1)
        target = jnp.clip(target, 0, F - 1)
        ref = wall.at[source, 1 - y, prows(0)]
        sem = s if wait else s + 1
        return rc(ref, ref, ds_sem.at[direction, s], dr_sem.at[direction, sem], "fs", target)

    def onward(direction):
        return z < F - 1 if direction == 0 else z > 0

    def arrives(direction, s):
        return z - s >= 0 if direction == 0 else z + s < F

    def rep_copy(source, p, j):
        ref = wall.at[source, y, prows(p)]
        return rc(ref, ref, ys_sem.at[source, p, j], yr_sem.at[source, p, j], "rep", rep_peer(j))

    def rep_arrival(source, p, j):
        ref = wall.at[source, lax.rem(y + R - j, R), prows(p)]
        return rc(ref, ref, ys_sem.at[source, p, j], yr_sem.at[source, p, j], "rep", rep_peer(j))

    def send_own(lo, hi):
        for p in range(lo, hi):
            for j in range(1, R):
                rep_copy(z, p, j).start()
            for d in (0, 1):

                @pl.when(onward(d))
                def _():
                    fs_copy(d, 0, p).start()

    def relay(s, lo, hi):
        if s >= F:
            return
        for p in range(lo, hi):
            for d in (0, 1):

                @pl.when(arrives(d, s))
                def _():
                    source = z - s if d == 0 else z + s
                    fs_copy(d, s, p, wait=True).wait_recv()
                    if s < F - 1:

                        @pl.when(onward(d))
                        def _():
                            fs_copy(d, s, p).start()

                    if not (plan.dup and p == 0):
                        for j in range(1, R):
                            rep_copy(source, p, j).start()

        if plan.dup and hi == NP:
            for d in (0, 1):

                @pl.when(arrives(d, s))
                def _():
                    dup_copy(d, s, wait=True).wait_recv()
                    if s < F - 1:

                        @pl.when(onward(d))
                        def _():
                            dup_copy(d, s).start()

    NH = (NP + 1) // 2
    send_own(0, NH)

    for i in (0, 1, 2):
        loads[i].wait()
    basis = jnp.dot(x[...], kfac[...], preferred_element_type=jnp.float32)
    partial[:, : plan.kc] = contract(basis, kcot[...])
    for i in (3, 4):
        loads[i].wait()
    basis = jnp.dot(x[...], vfac[...], preferred_element_type=jnp.float32)
    partial[:, plan.kc :] = contract(basis, vcot[...])

    H = plan.half
    ysend[...] = partial[...].astype(SCATTER_TYPE)
    for j in range(1, R):
        to = rep_peer(j)
        rc(ysend.at[pl.ds(to * H, H)], yrecv.at[j], rys.at[j], ryr.at[j], "rep", to).start()
    send_own(NH, NP)
    if plan.dup:
        rep_arrival(z, 0, 1).wait_recv()
        for d in (0, 1):

            @pl.when(onward(d))
            def _():
                dup_copy(d, 0).start()

    acc = partial[pl.ds(y * H, H), :]
    for j in range(1, R):
        rc(ysend.at[pl.ds(0, H)], yrecv.at[j], rys.at[j], ryr.at[j], "rep", rep_peer(j)).wait_recv()
        acc = acc + yrecv[j].astype(jnp.float32)
    half[...] = acc
    zsend[...] = acc.astype(SCATTER_TYPE)

    S, O = plan.slice, plan.owners

    def slice_copy(j):
        to = fs_peer(j)
        rows = pl.ds(jnp.minimum(to, O - 1) * S, S)
        return rc(zsend.at[rows], zrecv.at[j], rzs.at[j], rzr.at[j], "fs", to)

    for j in range(1, F):

        @pl.when(fs_peer(j) < O)
        def _():
            slice_copy(j).start()

    relay(1, 0, NH)

    mine = pl.ds(y * H + jnp.minimum(z, O - 1) * S, S)

    def sum_copy(j):
        return rc(total.at[mine], total.at[mine], gzs.at[j], gzr.at[j], "fs", fs_peer(j))

    @pl.when(z < O)
    def _():
        acc = half[pl.ds(jnp.minimum(z, O - 1) * S, S), :]
        for j in range(1, F):
            slice_copy(j).wait_recv()
            acc = acc + zrecv[j].astype(jnp.float32)
        total[mine, :] = acc.astype(GATHER_TYPE)
        for j in range(1, F):
            sum_copy(j).start()

    relay(1, NH, NP)

    for j in range(1, F):
        src = lax.rem(z + F - j, F)

        @pl.when(src < O)
        def _():
            rows = pl.ds(y * H + jnp.minimum(src, O - 1) * S, S)
            rc(total.at[rows], total.at[rows], gzs.at[j], gzr.at[j], "fs", fs_peer(j)).wait_recv()

    def half_copy(j):
        rows = pl.ds(y * H, H)
        return rc(total.at[rows], total.at[rows], gys.at[j], gyr.at[j], "rep", rep_peer(j))

    for j in range(1, R):
        half_copy(j).start()

    relay(2, 0, NH)

    for j in range(1, R):
        rows = pl.ds(lax.rem(y + R - j, R) * H, H)
        rc(total.at[rows], total.at[rows], gys.at[j], gyr.at[j], "rep", rep_peer(j)).wait_recv()

    proj = total[:, : plan.kc].astype(jnp.float32)
    first_new, second_new, normed = moments(proj, kf[...], ks[...])
    kf_out[...] = first_new
    ks_out[...] = second_new
    normed_out[:, : plan.kc] = normed
    squares = jnp.sum(normed * normed, axis=0, keepdims=True)
    squares = jnp.sum(squares, axis=1, keepdims=True)
    proj = total[:, plan.kc :].astype(jnp.float32)
    first_new, second_new, normed = moments(proj, vf[...], vs[...])
    vf_out[...] = first_new
    vs_out[...] = second_new
    normed_out[:, plan.kc :] = normed
    more = jnp.sum(normed * normed, axis=0, keepdims=True)
    squares = squares + jnp.sum(more, axis=1, keepdims=True)
    sq[t] = jnp.broadcast_to(squares, (8, 128))

    def sq_copy(j):
        return rc(sq.at[t], sq.at[t], ts.at[j], tr.at[j], "tp", tp_peer(j))

    for j in range(1, T):
        sq_copy(j).start()

    relay(2, NH, NP)

    for j in range(1, T):
        src = lax.rem(t + T - j, T)
        rc(sq.at[src], sq.at[src], ts.at[j], tr.at[j], "tp", tp_peer(j)).wait_recv()
    acc = sq[0]
    for i in range(1, T):
        acc = acc + sq[i]
    squares_out[...] = acc

    for s in range(3, F):
        relay(s, 0, NP)

    for source in range(F):
        for p in range(NP):
            for j in range(1, R):
                if plan.dup and p == 0:

                    @pl.when(z == source)
                    def _():
                        rep_copy(source, p, j).wait_send()
                else:
                    rep_arrival(source, p, j).wait_recv()
                    rep_copy(source, p, j).wait_send()
    for s in range(F - 1):
        for d in (0, 1):

            @pl.when(jnp.logical_and(arrives(d, s), onward(d)))
            def _():
                for p in range(NP):
                    fs_copy(d, s, p).wait_send()
                if plan.dup:
                    dup_copy(d, s).wait_send()
    for j in range(1, R):
        rc(ysend.at[pl.ds(0, H)], yrecv.at[j], rys.at[j], ryr.at[j], "rep", rep_peer(j)).wait_send()
        half_copy(j).wait_send()
    for j in range(1, F):

        @pl.when(fs_peer(j) < O)
        def _():
            slice_copy(j).wait_send()

        @pl.when(z < O)
        def _():
            sum_copy(j).wait_send()
    for j in range(1, T):
        sq_copy(j).wait_send()


def exchange(plan, *args):
    x, kcot, vcot, kfac, vfac = args[:5]
    F, R, T, NP, C = plan.F, plan.R, plan.T, plan.pieces, plan.cols
    f32 = jnp.float32
    vmem = pl.BlockSpec(memory_space=pltpu.VMEM)
    hbm = pl.BlockSpec(memory_space=pl.ANY)
    dma = pltpu.SemaphoreType.DMA
    rank = plan.rank
    out_shape = (
        jax.ShapeDtypeStruct((F, R, plan.rows, C), jnp.bfloat16),
        jax.ShapeDtypeStruct((rank, plan.kc), f32),
        jax.ShapeDtypeStruct((rank, plan.kc), f32),
        jax.ShapeDtypeStruct((rank, plan.vc), f32),
        jax.ShapeDtypeStruct((rank, plan.vc), f32),
        jax.ShapeDtypeStruct((rank, C), f32),
        jax.ShapeDtypeStruct((8, 128), f32),
    )
    scratch = [pltpu.VMEM(a.shape, a.dtype) for a in (x, kcot, vcot, kfac, vfac)]
    scratch += [
        pltpu.VMEM((rank, C), f32),
        pltpu.VMEM((rank, C), SCATTER_TYPE),
        pltpu.VMEM((R, plan.half, C), SCATTER_TYPE),
        pltpu.VMEM((plan.half, C), f32),
        pltpu.VMEM((plan.half, C), SCATTER_TYPE),
        pltpu.VMEM((F, plan.slice, C), SCATTER_TYPE),
        pltpu.VMEM((rank, C), GATHER_TYPE),
        pltpu.VMEM((T, 8, 128), f32),
        dma((5,)),
        dma((2, F, NP)),
        dma((2, F, NP)),
        dma((F, NP, R)),
        dma((F, NP, R)),
        dma((2, F)),
        dma((2, F)),
        dma((R,)), dma((R,)),
        dma((F,)), dma((F,)),
        dma((F,)), dma((F,)),
        dma((R,)), dma((R,)),
        dma((T,)), dma((T,)),
    ]
    return pl.pallas_call(
        functools.partial(kernel, plan),
        out_shape=out_shape,
        in_specs=[hbm] * 5 + [vmem] * 6,
        out_specs=[vmem] * 7,
        scratch_shapes=scratch,
        compiler_params=pltpu.CompilerParams(
            collective_id=0, has_side_effects=True, vmem_limit_bytes=48 * 1024 * 1024
        ),
    )(*args)


def body(mesh_shape, *args):
    (x, kcot, vcot, kfac, vfac, kw, vw, kf, ks, vf, vs) = args
    rows, key_cols = kw.shape
    value_cols = vw.shape[1]
    plan = Plan(mesh_shape, rows, kf.shape[0], key_cols, value_cols)
    wall, kf_new, ks_new, vf_new, vs_new, normed, squares = exchange(plan, *args)
    T = plan.T
    entries = jnp.float32(kf.size * T + vf.size * T)
    shrink = jnp.sqrt(entries / (entries + squares[0, 0]))

    row_offset = lax.axis_index(("fs", "rep")) * rows
    upper = normed.astype(jnp.bfloat16)
    lower = (normed - upper.astype(jnp.float32)).astype(jnp.bfloat16)

    def one(factor, weight, lo, hi):
        mine = lax.dynamic_slice_in_dim(factor, row_offset, rows, 0)
        step = jnp.dot(mine, upper[:, lo:hi], preferred_element_type=jnp.float32)
        step = step + jnp.dot(mine, lower[:, lo:hi], preferred_element_type=jnp.float32)
        step = shrink * step
        weight_new = weight - learn_rate * step
        everywhere = wall.reshape(-1, plan.cols)[:, lo:hi].astype(jnp.float32)
        full = jnp.dot(factor, upper[:, lo:hi], preferred_element_type=jnp.float32)
        copy = (everywhere - learn_rate * (shrink * full)).astype(jnp.bfloat16)
        return weight_new, step, copy

    k_new, k_step, k_copy = one(kfac, kw, 0, plan.kc)
    v_new, v_step, v_copy = one(vfac, vw, plan.kc, plan.cols)
    return (k_new, v_new, kf_new, ks_new, vf_new, vs_new, k_step, v_step, k_copy, v_copy)


def solution(mesh):
    rows = P(("fs", "rep"), "tp")
    cols = P(None, "tp")
    in_specs = (P(("fs", "rep"), None), rows, rows, P(), P(), rows, rows, cols, cols, cols, cols)
    out_specs = (rows, rows, cols, cols, cols, cols, rows, rows, cols, cols)
    return jax.shard_map(
        functools.partial(body, dict(mesh.shape)),
        mesh=mesh, in_specs=in_specs, out_specs=out_specs, check_vma=False,
    )
```

time: 226 us -> 126 us (0.56)
  waiting for transfers between devices: 180 us -> 0 us
  Pallas kernels: 0 us -> 78.8 us
  local copies, waits for them, and re-layouts: 6.12 us -> 29.3 us
  between operations: 15.9 us -> 1.45 us
  blocking collectives: 6.17 us -> 0 us
  other arithmetic: 4.39 us -> 0.07 us
  matrix products: 13 us -> 15.7 us
    all_gather x2 -> x0, waiting for transfers between devices: 102 us -> none  [the longest x1 61.2 us: body(): lax.all_gather(value_weight_new.astype(jnp.bfloat16), ('fs', 'rep'), axis...]
    pallas_call x0 -> x1, Pallas kernels: none -> 78.8 us  [exchange(): pl.pallas_call(functools.partial(kernel, plan), out_shape=out_shape, in_s...]
    psum x1 -> x0, waiting for transfers between devices: 77.9 us -> none  [body(): lax.psum((key_part, value_part), ('fs', 'rep'))]
    unnamed x28 -> x26, local copies, waits for them, and re-layouts: 6.12 us -> 25.6 us
    psum x1 -> x0, blocking collectives: 6.17 us -> none  [body(): squares = lax.psum(local_squares, 'tp')]
    reduce_sum x2 -> x0, other arithmetic: 4.39 us -> none  [the longest x1 2.2 us: body(): jnp.sum(value_normed * value_normed)]
    slice x0 -> x3, local copies, waits for them, and re-layouts: none -> 3.67 us  [the longest x2 3.16 us: one(): everywhere = wall.reshape(-1, plan.cols)[:, lo:hi].astype(jnp.float32)]
    dot_general x8 -> x6, matrix products: 13 us -> 15.7 us  [the longest x2 8.87 us: one(): full = jnp.dot(factor, upper[:, lo:hi], preferred_element_type=jnp.float32)]
  transfers between devices with their start and end apart: 3 -> 0, of which waited for: 3 -> 0; matrix products, arithmetic and copies ran while one was open for 1% -> 0% of each run, Pallas kernels for 0% -> 0%
where the time goes in v1:
time: 126 us; the launch traced here: 125 us
  Pallas kernels  78.8 us (63%)
  local copies, waits for them, and re-layouts  29.3 us (23%)
  matrix products  15.7 us (12%)
  between operations  1.45 us (1%)
    pallas_call x1, Pallas kernels, exchange(): pl.pallas_call(functools.partial(kernel, plan), out_shape=out_shape, in_s...  78.8 us
    unnamed x26, local copies, waits for them, and re-layouts  25.6 us
    dot_general x2, matrix products, one(): full = jnp.dot(factor, upper[:, lo:hi], preferred_element_type=jnp.float32)  8.87 us
    dot_general x2, matrix products, one(): jnp.dot(mine, lower[:, lo:hi], preferred_element_type=jnp.float32)  4.53 us
    slice x2, local copies, waits for them, and re-layouts, one(): everywhere = wall.reshape(-1, plan.cols)[:, lo:hi].astype(jnp.float32)  3.16 us

profile of v1, /device:TPU:0, one launch (start us, length us, event | category | flops | bytes accessed | tf_op | source)
XLA Modules:
  0.0 125.3 jit_solution(3199326986669899140)
XLA Ops:
  0.7 0.0 copy-start
  0.7 1.1 copy-done
  1.8 0.0 copy-start.1
  1.8 1.0 copy-done.1
  2.8 0.0 copy-start.2
  2.8 1.1 copy-done.2
  3.9 0.0 copy-start.3
  3.9 1.0 copy-done.3
  4.9 0.0 copy-start.4
  4.9 1.0 copy-done.4
  6.0 0.0 copy-start.5
  6.0 1.0 copy-done.5
  6.9 0.0 copy-start.6
  6.9 0.9 copy-done.6
  7.9 0.0 copy-start.7
  7.9 0.9 copy-done.7
  8.8 78.8 %shard_map.186 = (bf16[4,2,384,768]{3,2,1,0:T(8,128)(2,1)}, f32[256,256]{1,0:T(8,128)S(1)}, f32[256,256]{1,0:T(8,128)S(1)}, f32[256,512]{1,0:T(8,128)S(1)}, f32[...) custom-call(bf16[640,3072]{1,0:T(8,128)(2,1)} %x_hbm.1, bf16[640,256]{1,0:T(8,128)(2,1)S(1)} %copy-done.5, ...), custom_call_target="tpu_custom_call" | custom-call | tf_op jit(solution)/shard_map/pallas_call | solution.py:380
  87.6 0.5 slice.23
  88.8 0.1 subtract_convert_fusion
  88.9 1.1 fusion.14
  90.1 0.0 copy-start.8
  90.1 2.2 %multiply_subtract_fusion.1 = (f32[384,256]{1,0:T(8,128)}, f32[384,256]{1,0:T(8,128)}) fusion(f32[384,256]{1,0:T(8,128)S(1)} %copy-done.1, f32[384,256]{1,0:T(8,128)S(1)} %fusion.14, bf16[256,768]{1,0:T(8,128)(2,1)S(1)} %get-tuple-element.34, bf16[3072,256]{1,0:T(8,128)(2,1)} %kfac_hbm.1, s32[]{:T(128)S(6)} %select_n.4, f32[]{:T(128)} %bitcast), kind=kOutput, calls=%fused_computation.13 | convolution fusion | flops 50724864 | bytes 1901060 | tf_op jit(solution)/shard_map/dot_general | solution.py:409
  92.2 1.2 fusion.9
  93.4 2.3 %multiply_subtract_fusion = (f32[384,512]{1,0:T(8,128)}, f32[384,512]{1,0:T(8,128)}) fusion(f32[384,512]{1,0:T(8,128)S(1)} %copy-done, f32[384,512]{1,0:T(8,128)S(1)} %fusion.9, bf16[256,768]{1,0:T(8,128)(2,1)S(1)} %get-tuple-element.34, bf16[3072,256]{1,0:T(8,128)(2,1)} %vfac_hbm.1, s32[]{:T(128)S(6)} %select_n.4, f32[]{:T(128)} %bitcast), kind=kOutput, calls=%fused_computation.11 | convolution fusion | flops 101449728 | bytes 3604996 | tf_op jit(solution)/shard_map/dot_general | solution.py:409
  95.8 0.0 copy-done.8
  95.8 1.2 slice.34
  97.0 1.9 %slice.35 = bf16[3072,512]{1,0:T(8,128)(2,1)} slice(bf16[3072,768]{1,0:T(8,128)(2,1)S(1)} %bitcast.15), slice={[0:3072], [256:768]} | slice | bytes 6291456 | tf_op jit(solution)/shard_map/slice | solution.py:412
  98.9 4.6 %copy.26 = bf16[3072,512]{0,1:T(8,128)(2,1)} copy(bf16[3072,512]{1,0:T(8,128)(2,1)} %slice.35) | data formatting | bytes 6291456
  103.6 5.1 %fusion = bf16[3072,512]{0,1:T(8,128)(2,1)} fusion(bf16[3072,512]{0,1:T(8,128)(2,1)} %copy.26, bf16[3072,256]{1,0:T(8,128)(2,1)} %vfac_hbm.1, f32[]{:T(128)} %bitcast, bf16[256,768]{1,0:T(8,128)(2,1)S(1)} %get-tuple-element.35), kind=kOutput, calls=%fused_computation.1 | convolution fusion | flops 813170688 | bytes 8126468 | tf_op jit(solution)/shard_map/dot_general | solution.py:413
  108.7 4.6 %copy.24 = bf16[3072,512]{1,0:T(8,128)(2,1)} copy(bf16[3072,512]{0,1:T(8,128)(2,1)} %fusion) | data formatting | bytes 6291456
  113.4 2.6 %copy.25 = bf16[3072,256]{0,1:T(8,128)(2,1)} copy(bf16[3072,256]{1,0:T(8,128)(2,1)} %slice.34) | data formatting | bytes 3145728
  116.0 3.7 %fusion.4 = bf16[3072,256]{0,1:T(8,128)(2,1)} fusion(bf16[3072,256]{1,0:T(8,128)(2,1)} %kfac_hbm.1, bf16[3072,256]{0,1:T(8,128)(2,1)} %copy.25, f32[]{:T(128)} %bitcast, bf16[256,768]{1,0:T(8,128)(2,1)S(1)} %get-tuple-element.35), kind=kOutput, calls=%fused_computation.6 | convolution fusion | flops 406585344 | bytes 4849668 | tf_op jit(solution)/shard_map/dot_general | solution.py:413
  119.7 2.6 %copy.23 = bf16[3072,256]{1,0:T(8,128)(2,1)} copy(bf16[3072,256]{0,1:T(8,128)(2,1)} %fusion.4) | data formatting | bytes 3145728
  122.3 0.7 copy.31
  123.0 0.7 copy.32
  123.7 0.8 copy.33
  124.5 0.8 copy.34
Async XLA Ops:
  0.7 1.1 copy-start
  1.8 1.0 copy-start.1
  2.8 1.1 copy-start.2
  3.9 1.0 copy-start.3
  4.9 1.0 copy-start.4
  6.0 1.0 copy-start.5
  6.9 0.9 copy-start.6
  7.9 0.9 copy-start.7
  90.1 5.7 %copy-start.8 = (bf16[4,2,384,768]{3,2,1,0:T(8,128)(2,1)S(1)}, bf16[4,2,384,768]{3,2,1,0:T(8,128)(2,1)}, u32[]{:S(2)}) copy-start(bf16[4,2,384,768]{3,2,1,0:T(8,128)(2,1)} %get-tuple-element.23) | copy-start | bytes 14155780

commit v2 on v1

--- a/solution.py
+++ b/solution.py
@@ -53,9 +53,10 @@
 
 def kernel(
     plan,
-    x_hbm, kcot_hbm, vcot_hbm, kfac_hbm, vfac_hbm, kw, vw, kf, ks, vf, vs,
-    wall, kf_out, ks_out, vf_out, vs_out, normed_out, squares_out,
-    x, kcot, vcot, kfac, vfac, partial, ysend, yrecv, half, zsend, zrecv, total, sq,
+    x_hbm, kcot_hbm, vcot_hbm, kfac_hbm, vfac_hbm, kw_hbm, vw_hbm, kf_hbm, ks_hbm, vf_hbm, vs_hbm,
+    wall, total, squares_out,
+    x, kcot, vcot, kfac, vfac, kw, vw, kf, ks, vf, vs,
+    partial, ysend, yrecv, half, zsend, zrecv, sq,
     load_sem, zs_sem, zr_sem, ys_sem, yr_sem, ds_sem, dr_sem,
     rys, ryr, rzs, rzr, gzs, gzr, gys, gyr, ts, tr,
 ):
@@ -68,11 +69,15 @@
     loads = [
         pltpu.make_async_copy(s, d, load_sem.at[i])
         for i, (s, d) in enumerate(
-            ((x_hbm, x), (kfac_hbm, kfac), (kcot_hbm, kcot), (vfac_hbm, vfac), (vcot_hbm, vcot))
+            (
+                (x_hbm, x), (kfac_hbm, kfac), (kcot_hbm, kcot), (vfac_hbm, vfac), (vcot_hbm, vcot),
+                (kw_hbm, kw), (vw_hbm, vw),
+                (kf_hbm, kf), (ks_hbm, ks), (vf_hbm, vf), (vs_hbm, vs),
+            )
         )
     ]
-    for c in loads:
-        c.start()
+    for i in (5, 6, 0, 1, 2, 3, 4, 7, 8, 9, 10):
+        loads[i].start()
 
     def fs_peer(j):
         return lax.rem(z + j, F)
@@ -89,6 +94,8 @@
             pl.semaphore_signal(barrier, 1, device_id={axis: peer(j)}, device_id_type=MESH)
 
     own = wall.at[z, y]
+    for i in (5, 6):
+        loads[i].wait()
     own[:, : plan.kc] = kw[...].astype(jnp.bfloat16)
     own[:, plan.kc :] = vw[...].astype(jnp.bfloat16)
     pl.semaphore_wait(barrier, F + R + T - 3)
@@ -266,20 +273,14 @@
         rows = pl.ds(lax.rem(y + R - j, R) * H, H)
         rc(total.at[rows], total.at[rows], gys.at[j], gyr.at[j], "rep", rep_peer(j)).wait_recv()
 
-    proj = total[:, : plan.kc].astype(jnp.float32)
-    first_new, second_new, normed = moments(proj, kf[...], ks[...])
-    kf_out[...] = first_new
-    ks_out[...] = second_new
-    normed_out[:, : plan.kc] = normed
-    squares = jnp.sum(normed * normed, axis=0, keepdims=True)
-    squares = jnp.sum(squares, axis=1, keepdims=True)
-    proj = total[:, plan.kc :].astype(jnp.float32)
-    first_new, second_new, normed = moments(proj, vf[...], vs[...])
-    vf_out[...] = first_new
-    vs_out[...] = second_new
-    normed_out[:, plan.kc :] = normed
-    more = jnp.sum(normed * normed, axis=0, keepdims=True)
-    squares = squares + jnp.sum(more, axis=1, keepdims=True)
+    for i in (7, 8, 9, 10):
+        loads[i].wait()
+    squares = jnp.zeros((1, 1), jnp.float32)
+    for lo, hi, first, second in ((0, plan.kc, kf, ks), (plan.kc, plan.cols, vf, vs)):
+        proj = total[:, lo:hi].astype(jnp.float32)
+        _, _, normed = moments(proj, first[...], second[...])
+        line = jnp.sum(normed * normed, axis=0, keepdims=True)
+        squares = squares + jnp.sum(line, axis=1, keepdims=True)
     sq[t] = jnp.broadcast_to(squares, (8, 128))
 
     def sq_copy(j):
@@ -338,23 +339,18 @@
 
 
 def exchange(plan, *args):
-    x, kcot, vcot, kfac, vfac = args[:5]
     F, R, T, NP, C = plan.F, plan.R, plan.T, plan.pieces, plan.cols
     f32 = jnp.float32
     vmem = pl.BlockSpec(memory_space=pltpu.VMEM)
-    hbm = pl.BlockSpec(memory_space=pl.ANY)
+    hbm = pl.BlockSpec(memory_space=pltpu.HBM)
     dma = pltpu.SemaphoreType.DMA
     rank = plan.rank
     out_shape = (
         jax.ShapeDtypeStruct((F, R, plan.rows, C), jnp.bfloat16),
-        jax.ShapeDtypeStruct((rank, plan.kc), f32),
-        jax.ShapeDtypeStruct((rank, plan.kc), f32),
-        jax.ShapeDtypeStruct((rank, plan.vc), f32),
-        jax.ShapeDtypeStruct((rank, plan.vc), f32),
-        jax.ShapeDtypeStruct((rank, C), f32),
+        jax.ShapeDtypeStruct((rank, C), GATHER_TYPE),
         jax.ShapeDtypeStruct((8, 128), f32),
     )
-    scratch = [pltpu.VMEM(a.shape, a.dtype) for a in (x, kcot, vcot, kfac, vfac)]
+    scratch = [pltpu.VMEM(a.shape, a.dtype) for a in args]
     scratch += [
         pltpu.VMEM((rank, C), f32),
         pltpu.VMEM((rank, C), SCATTER_TYPE),
@@ -362,9 +358,8 @@
         pltpu.VMEM((plan.half, C), f32),
         pltpu.VMEM((plan.half, C), SCATTER_TYPE),
         pltpu.VMEM((F, plan.slice, C), SCATTER_TYPE),
-        pltpu.VMEM((rank, C), GATHER_TYPE),
         pltpu.VMEM((T, 8, 128), f32),
-        dma((5,)),
+        dma((11,)),
         dma((2, F, NP)),
         dma((2, F, NP)),
         dma((F, NP, R)),
@@ -380,13 +375,73 @@
     return pl.pallas_call(
         functools.partial(kernel, plan),
         out_shape=out_shape,
-        in_specs=[hbm] * 5 + [vmem] * 6,
-        out_specs=[vmem] * 7,
+        in_specs=[hbm] * 11,
+        out_specs=[vmem] * 3,
         scratch_shapes=scratch,
         compiler_params=pltpu.CompilerParams(
-            collective_id=0, has_side_effects=True, vmem_limit_bytes=48 * 1024 * 1024
+            collective_id=0, has_side_effects=True, vmem_limit_bytes=28 * 1024 * 1024
         ),
     )(*args)
+
+
+BLOCKS = 8
+
+
+def finish(
+    plan, kfac, vfac, kw, vw, kf, ks, vf, vs, wall, total, squares,
+    kw_out, vw_out, kf_out, ks_out, vf_out, vs_out, kstep_out, vstep_out, kcopy_out, vcopy_out,
+    kw_new, vw_new, kf_new, ks_new, vf_new, vs_new, kstep, vstep, kcopy, vcopy, sem, copy_sem,
+):
+    me = lax.axis_index("fs") * plan.R + lax.axis_index("rep")
+    mine = pl.ds(me * plan.rows, plan.rows)
+    entries = jnp.float32(plan.rank * plan.cols * plan.T)
+    shrink = jnp.sqrt(entries / (entries + squares[0:1, 0:1]))
+    depth = kfac.shape[0] // BLOCKS
+
+    def out(i, src, dst):
+        c = pltpu.make_async_copy(src, dst, sem.at[i])
+        c.start()
+        return c
+
+    sides = (
+        (0, plan.kc, kfac, kw, kf, ks, (kf_new, ks_new, kstep, kw_new), (kf_out, ks_out, kstep_out, kw_out)),
+        (plan.kc, plan.cols, vfac, vw, vf, vs, (vf_new, vs_new, vstep, vw_new), (vf_out, vs_out, vstep_out, vw_out)),
+    )
+    pending, uppers, lowers = [], [], []
+    for k, (lo, hi, _, _, first, second, news, outs) in enumerate(sides):
+        proj = total[:, lo:hi].astype(jnp.float32)
+        first_new, second_new, normed = moments(proj, first[...], second[...])
+        news[0][...] = first_new
+        news[1][...] = second_new
+        upper = normed.astype(jnp.bfloat16)
+        uppers.append(upper)
+        lowers.append((normed - upper.astype(jnp.float32)).astype(jnp.bfloat16))
+        for i in (0, 1):
+            pending.append(out(4 * k + i, news[i], outs[i]))
+
+    for b in range(BLOCKS):
+        rows = pl.ds(b * depth, depth)
+        for k, (dst, dst_out) in enumerate(((kcopy, kcopy_out), (vcopy, vcopy_out))):
+            lo, hi, factor = sides[k][:3]
+            full = jnp.dot(factor[rows, :], uppers[k], preferred_element_type=jnp.float32)
+            step = shrink * full
+            dst[rows, :] = (wall[rows, lo:hi].astype(jnp.float32) - learn_rate * step).astype(
+                jnp.bfloat16
+            )
+            c = pltpu.make_async_copy(dst.at[rows], dst_out.at[rows], copy_sem.at[k, b])
+            c.start()
+            pending.append(c)
+
+    for k, (lo, hi, factor, weight, _, _, news, outs) in enumerate(sides):
+        part = factor[mine, :]
+        step = jnp.dot(part, uppers[k], preferred_element_type=jnp.float32)
+        step = shrink * (step + jnp.dot(part, lowers[k], preferred_element_type=jnp.float32))
+        news[2][...] = step
+        news[3][...] = weight[...] - learn_rate * step
+        for i in (2, 3):
+            pending.append(out(4 * k + i, news[i], outs[i]))
+    for c in pending:
+        c.wait()
 
 
 def body(mesh_shape, *args):
@@ -394,29 +449,21 @@
     rows, key_cols = kw.shape
     value_cols = vw.shape[1]
     plan = Plan(mesh_shape, rows, kf.shape[0], key_cols, value_cols)
-    wall, kf_new, ks_new, vf_new, vs_new, normed, squares = exchange(plan, *args)
-    T = plan.T
-    entries = jnp.float32(kf.size * T + vf.size * T)
-    shrink = jnp.sqrt(entries / (entries + squares[0, 0]))
-
-    row_offset = lax.axis_index(("fs", "rep")) * rows
-    upper = normed.astype(jnp.bfloat16)
-    lower = (normed - upper.astype(jnp.float32)).astype(jnp.bfloat16)
-
-    def one(factor, weight, lo, hi):
-        mine = lax.dynamic_slice_in_dim(factor, row_offset, rows, 0)
-        step = jnp.dot(mine, upper[:, lo:hi], preferred_element_type=jnp.float32)
-        step = step + jnp.dot(mine, lower[:, lo:hi], preferred_element_type=jnp.float32)
-        step = shrink * step
-        weight_new = weight - learn_rate * step
-        everywhere = wall.reshape(-1, plan.cols)[:, lo:hi].astype(jnp.float32)
-        full = jnp.dot(factor, upper[:, lo:hi], preferred_element_type=jnp.float32)
-        copy = (everywhere - learn_rate * (shrink * full)).astype(jnp.bfloat16)
-        return weight_new, step, copy
-
-    k_new, k_step, k_copy = one(kfac, kw, 0, plan.kc)
-    v_new, v_step, v_copy = one(vfac, vw, plan.kc, plan.cols)
-    return (k_new, v_new, kf_new, ks_new, vf_new, vs_new, k_step, v_step, k_copy, v_copy)
+    wall, total, squares = exchange(plan, *args)
+    wall = wall.reshape(-1, plan.cols)
+    like = [jax.ShapeDtypeStruct(a.shape, a.dtype) for a in (kw, vw, kf, ks, vf, vs, kw, vw)]
+    depth = kfac.shape[0]
+    like += [jax.ShapeDtypeStruct((depth, c), jnp.bfloat16) for c in (key_cols, value_cols)]
+    vmem = pl.BlockSpec(memory_space=pltpu.VMEM)
+    return pl.pallas_call(
+        functools.partial(finish, plan),
+        out_shape=like,
+        in_specs=[vmem] * 11,
+        out_specs=[pl.BlockSpec(memory_space=pl.ANY)] * 10,
+        scratch_shapes=[pltpu.VMEM(a.shape, a.dtype) for a in like]
+        + [pltpu.SemaphoreType.DMA((8,)), pltpu.SemaphoreType.DMA((2, BLOCKS))],
+        compiler_params=pltpu.CompilerParams(vmem_limit_bytes=20 * 1024 * 1024),
+    )(kfac, vfac, kw, vw, kf, ks, vf, vs, wall, total, squares)
 
 
 def solution(mesh):

time: 126 us -> 95.7 us (0.76)
  local copies, waits for them, and re-layouts: 29.3 us -> 13.1 us
  matrix products: 15.7 us -> 0 us
  Pallas kernels: 78.8 us -> 81.4 us
    dot_general x6 -> x0, matrix products: 15.7 us -> none  [the longest x2 8.87 us: one(): full = jnp.dot(factor, upper[:, lo:hi], preferred_element_type=jnp.float32)]
    unnamed x26 -> x22, local copies, waits for them, and re-layouts: 25.6 us -> 13.1 us
    pallas_call x0 -> x1, Pallas kernels: none -> 4.58 us  [body(): pl.pallas_call(functools.partial(finish, plan), out_shape=like, in_specs=...]
    slice x3 -> x0, local copies, waits for them, and re-layouts: 3.67 us -> none  [the longest x2 3.16 us: one(): everywhere = wall.reshape(-1, plan.cols)[:, lo:hi].astype(jnp.float32)]
    pallas_call x1, Pallas kernels: 78.8 us -> 76.9 us  [exchange(): pl.pallas_call(functools.partial(kernel, plan), out_shape=out_shape, in_s...]
where the time goes in v2:
time: 95.7 us; the launch traced here: 95.2 us
  Pallas kernels  81.4 us (85%)
  local copies, waits for them, and re-layouts  13.1 us (14%)
    pallas_call x1, Pallas kernels, exchange(): pl.pallas_call(functools.partial(kernel, plan), out_shape=out_shape, in_s...  76.9 us
    unnamed x22, local copies, waits for them, and re-layouts  13.1 us
    pallas_call x1, Pallas kernels, body(): pl.pallas_call(functools.partial(finish, plan), out_shape=like, in_specs=...  4.58 us

profile of v2, /device:TPU:0, one launch (start us, length us, event | category | flops | bytes accessed | tf_op | source)
XLA Modules:
  0.0 95.2 jit_solution(7687692411162709314)
XLA Ops:
  0.6 0.0 copy-start
  0.7 1.4 %copy-done = bf16[3072,256]{1,0:T(8,128)(2,1)S(1)} copy-done((bf16[3072,256]{1,0:T(8,128)(2,1)S(1)}, bf16[3072,256]{1,0:T(8,128)(2,1)}, u32[]{:S(2)}) %copy-start) | copy-done | bytes 1572888
  2.1 0.0 copy-start.1
  2.1 1.4 %copy-done.1 = bf16[3072,256]{1,0:T(8,128)(2,1)S(1)} copy-done((bf16[3072,256]{1,0:T(8,128)(2,1)S(1)}, bf16[3072,256]{1,0:T(8,128)(2,1)}, u32[]{:S(2)}) %copy-start.1) | copy-done | bytes 1572888
  3.5 0.0 copy-start.2
  3.5 2.1 %copy-done.2 = bf16[640,3072]{1,0:T(8,128)(2,1)S(1)} copy-done((bf16[640,3072]{1,0:T(8,128)(2,1)S(1)}, bf16[640,3072]{1,0:T(8,128)(2,1)}, u32[]{:S(2)}) %copy-start.2) | copy-done | bytes 3932184
  5.6 0.0 copy-start.3
  5.6 1.1 %copy-done.3 = f32[384,512]{1,0:T(8,128)S(1)} copy-done((f32[384,512]{1,0:T(8,128)S(1)}, f32[384,512]{1,0:T(8,128)}, u32[]{:S(2)}) %copy-start.3) | copy-done | bytes 786456
  6.7 0.0 copy-start.4
  6.7 1.0 %copy-done.4 = f32[256,512]{1,0:T(8,128)S(1)} copy-done((f32[256,512]{1,0:T(8,128)S(1)}, f32[256,512]{1,0:T(8,128)}, u32[]{:S(2)}) %copy-start.4) | copy-done | bytes 524312
  7.8 0.0 copy-start.5
  7.8 1.0 %copy-done.5 = f32[256,512]{1,0:T(8,128)S(1)} copy-done((f32[256,512]{1,0:T(8,128)S(1)}, f32[256,512]{1,0:T(8,128)}, u32[]{:S(2)}) %copy-start.5) | copy-done | bytes 524312
  8.8 0.0 copy-start.6
  8.8 1.0 %copy-done.6 = f32[384,256]{1,0:T(8,128)S(1)} copy-done((f32[384,256]{1,0:T(8,128)S(1)}, f32[384,256]{1,0:T(8,128)}, u32[]{:S(2)}) %copy-start.6) | copy-done | bytes 393240
  9.8 0.0 copy-start.7
  9.8 0.9 copy-done.7
  10.7 0.0 copy-start.8
  10.7 0.9 copy-done.8
  11.7 0.0 copy-start.9
  11.7 1.1 %copy-done.9 = bf16[640,512]{1,0:T(8,128)(2,1)S(1)} copy-done((bf16[640,512]{1,0:T(8,128)(2,1)S(1)}, bf16[640,512]{1,0:T(8,128)(2,1)}, u32[]{:S(2)}) %copy-start.9) | copy-done | bytes 655384
  12.8 0.0 copy-start.10
  12.8 1.0 %copy-done.10 = bf16[640,256]{1,0:T(8,128)(2,1)S(1)} copy-done((bf16[640,256]{1,0:T(8,128)(2,1)S(1)}, bf16[640,256]{1,0:T(8,128)(2,1)}, u32[]{:S(2)}) %copy-start.10) | copy-done | bytes 327704
  13.8 76.9 %shard_map.186 = (bf16[4,2,384,768]{3,2,1,0:T(8,128)(2,1)S(1)}, f32[256,768]{1,0:T(8,128)S(1)}, f32[8,128]{1,0:T(8,128)S(1)}) custom-call(bf16[640,3072]{1,0:T(8,128)(2,1)S(1)} %copy-done.2, bf16[640,256]{1,0:T(8,128)(2,1)S(1)} %copy-done.10, bf16[640,512]{1,0:T(8,128)(2,1)S(1)} %copy-done.9, bf16[3072,256]{1,0:T(8,128)(2,1)S(1)} %copy-done, ...), custom_call_target="tpu_custom_call" | custom-call | tf_op jit(solution)/shard_map/pallas_call | solution.py:375
  90.6 4.6 %shard_map.187 = (f32[384,256]{1,0:T(8,128)}, f32[384,512]{1,0:T(8,128)}, f32[256,256]{1,0:T(8,128)}, f32[256,256]{1,0:T(8,128)}, f32[256,512]{1,0:T(8,128)}, /*...) custom-call(bf16[3072,256]{1,0:T(8,128)(2,1)S(1)} %copy-done, ...), custom_call_target="tpu_custom_call" | custom-call | tf_op jit(solution)/shard_map/pallas_call | solution.py:458
Async XLA Ops:
  0.6 1.4 %copy-start = (bf16[3072,256]{1,0:T(8,128)(2,1)S(1)}, bf16[3072,256]{1,0:T(8,128)(2,1)}, u32[]{:S(2)}) copy-start(bf16[3072,256]{1,0:T(8,128)(2,1)} %kfac.1) | copy-start | bytes 4718596
  2.1 1.4 %copy-start.1 = (bf16[3072,256]{1,0:T(8,128)(2,1)S(1)}, bf16[3072,256]{1,0:T(8,128)(2,1)}, u32[]{:S(2)}) copy-start(bf16[3072,256]{1,0:T(8,128)(2,1)} %vfac.1) | copy-start | bytes 4718596
  3.5 2.1 %copy-start.2 = (bf16[640,3072]{1,0:T(8,128)(2,1)S(1)}, bf16[640,3072]{1,0:T(8,128)(2,1)}, u32[]{:S(2)}) copy-start(bf16[640,3072]{1,0:T(8,128)(2,1)} %x_hbm.1) | copy-start | bytes 11796484
  5.6 1.1 %copy-start.3 = (f32[384,512]{1,0:T(8,128)S(1)}, f32[384,512]{1,0:T(8,128)}, u32[]{:S(2)}) copy-start(f32[384,512]{1,0:T(8,128)} %vw.1) | copy-start | bytes 2359300
  6.7 1.0 %copy-start.4 = (f32[256,512]{1,0:T(8,128)S(1)}, f32[256,512]{1,0:T(8,128)}, u32[]{:S(2)}) copy-start(f32[256,512]{1,0:T(8,128)} %vf.1) | copy-start | bytes 1572868
  7.8 1.0 %copy-start.5 = (f32[256,512]{1,0:T(8,128)S(1)}, f32[256,512]{1,0:T(8,128)}, u32[]{:S(2)}) copy-start(f32[256,512]{1,0:T(8,128)} %vs.1) | copy-start | bytes 1572868
  8.8 1.0 %copy-start.6 = (f32[384,256]{1,0:T(8,128)S(1)}, f32[384,256]{1,0:T(8,128)}, u32[]{:S(2)}) copy-start(f32[384,256]{1,0:T(8,128)} %kw.1) | copy-start | bytes 1179652
  9.8 0.9 copy-start.7
  10.7 0.9 copy-start.8
  11.7 1.1 %copy-start.9 = (bf16[640,512]{1,0:T(8,128)(2,1)S(1)}, bf16[640,512]{1,0:T(8,128)(2,1)}, u32[]{:S(2)}) copy-start(bf16[640,512]{1,0:T(8,128)(2,1)} %vcot_hbm.1) | copy-start | bytes 1966084
  12.8 1.0 %copy-start.10 = (bf16[640,256]{1,0:T(8,128)(2,1)S(1)}, bf16[640,256]{1,0:T(8,128)(2,1)}, u32[]{:S(2)}) copy-start(bf16[640,256]{1,0:T(8,128)(2,1)} %kcot_hbm.1) | copy-start | bytes 983044

commit v3 on v2

--- a/solution.py
+++ b/solution.py
@@ -13,8 +13,9 @@
 epsilon = 1e-08
 learn_rate = 0.01
 
-SCATTER_TYPE = jnp.float32
-GATHER_TYPE = jnp.float32
+REP_TYPE = jnp.bfloat16
+FS_TYPE = jnp.float32
+GATHER_TYPE = jnp.bfloat16
 MESH = pl.DeviceIdType.MESH
 
 
@@ -54,8 +55,8 @@
 def kernel(
     plan,
     x_hbm, kcot_hbm, vcot_hbm, kfac_hbm, vfac_hbm, kw_hbm, vw_hbm, kf_hbm, ks_hbm, vf_hbm, vs_hbm,
-    wall, total, squares_out,
-    x, kcot, vcot, kfac, vfac, kw, vw, kf, ks, vf, vs,
+    wall, total, squares_out, kfac, vfac, kw, vw, kf, ks, vf, vs,
+    x, kcot, vcot,
     partial, ysend, yrecv, half, zsend, zrecv, sq,
     load_sem, zs_sem, zr_sem, ys_sem, yr_sem, ds_sem, dr_sem,
     rys, ryr, rzs, rzr, gzs, gzr, gys, gyr, ts, tr,
@@ -200,7 +201,7 @@
     partial[:, plan.kc :] = contract(basis, vcot[...])
 
     H = plan.half
-    ysend[...] = partial[...].astype(SCATTER_TYPE)
+    ysend[...] = partial[...].astype(REP_TYPE)
     for j in range(1, R):
         to = rep_peer(j)
         rc(ysend.at[pl.ds(to * H, H)], yrecv.at[j], rys.at[j], ryr.at[j], "rep", to).start()
@@ -218,7 +219,7 @@
         rc(ysend.at[pl.ds(0, H)], yrecv.at[j], rys.at[j], ryr.at[j], "rep", rep_peer(j)).wait_recv()
         acc = acc + yrecv[j].astype(jnp.float32)
     half[...] = acc
-    zsend[...] = acc.astype(SCATTER_TYPE)
+    zsend[...] = acc.astype(FS_TYPE)
 
     S, O = plan.slice, plan.owners
 
@@ -267,7 +268,8 @@
     for j in range(1, R):
         half_copy(j).start()
 
-    relay(2, 0, NH)
+    for s in range(2, F):
+        relay(s, 0, NP)
 
     for j in range(1, R):
         rows = pl.ds(lax.rem(y + R - j, R) * H, H)
@@ -289,8 +291,6 @@
     for j in range(1, T):
         sq_copy(j).start()
 
-    relay(2, NH, NP)
-
     for j in range(1, T):
         src = lax.rem(t + T - j, T)
         rc(sq.at[src], sq.at[src], ts.at[j], tr.at[j], "tp", tp_peer(j)).wait_recv()
@@ -298,9 +298,6 @@
     for i in range(1, T):
         acc = acc + sq[i]
     squares_out[...] = acc
-
-    for s in range(3, F):
-        relay(s, 0, NP)
 
     for source in range(F):
         for p in range(NP):
@@ -349,15 +346,15 @@
         jax.ShapeDtypeStruct((F, R, plan.rows, C), jnp.bfloat16),
         jax.ShapeDtypeStruct((rank, C), GATHER_TYPE),
         jax.ShapeDtypeStruct((8, 128), f32),
-    )
-    scratch = [pltpu.VMEM(a.shape, a.dtype) for a in args]
+    ) + tuple(jax.ShapeDtypeStruct(a.shape, a.dtype) for a in args[3:])
+    scratch = [pltpu.VMEM(a.shape, a.dtype) for a in args[:3]]
     scratch += [
         pltpu.VMEM((rank, C), f32),
-        pltpu.VMEM((rank, C), SCATTER_TYPE),
-        pltpu.VMEM((R, plan.half, C), SCATTER_TYPE),
+        pltpu.VMEM((rank, C), REP_TYPE),
+        pltpu.VMEM((R, plan.half, C), REP_TYPE),
         pltpu.VMEM((plan.half, C), f32),
-        pltpu.VMEM((plan.half, C), SCATTER_TYPE),
-        pltpu.VMEM((F, plan.slice, C), SCATTER_TYPE),
+        pltpu.VMEM((plan.half, C), FS_TYPE),
+        pltpu.VMEM((F, plan.slice, C), FS_TYPE),
         pltpu.VMEM((T, 8, 128), f32),
         dma((11,)),
         dma((2, F, NP)),
@@ -376,12 +373,12 @@
         functools.partial(kernel, plan),
         out_shape=out_shape,
         in_specs=[hbm] * 11,
-        out_specs=[vmem] * 3,
+        out_specs=[vmem] * 11,
         scratch_shapes=scratch,
         compiler_params=pltpu.CompilerParams(
-            collective_id=0, has_side_effects=True, vmem_limit_bytes=28 * 1024 * 1024
+            collective_id=0, has_side_effects=True, vmem_limit_bytes=40 * 1024 * 1024
         ),
-    )(*args)
+    )(*(pltpu.with_memory_space_constraint(a, pltpu.HBM) for a in args))
 
 
 BLOCKS = 8
@@ -449,7 +446,7 @@
     rows, key_cols = kw.shape
     value_cols = vw.shape[1]
     plan = Plan(mesh_shape, rows, kf.shape[0], key_cols, value_cols)
-    wall, total, squares = exchange(plan, *args)
+    wall, total, squares, *held = exchange(plan, *args)
     wall = wall.reshape(-1, plan.cols)
     like = [jax.ShapeDtypeStruct(a.shape, a.dtype) for a in (kw, vw, kf, ks, vf, vs, kw, vw)]
     depth = kfac.shape[0]
@@ -463,7 +460,7 @@
         scratch_shapes=[pltpu.VMEM(a.shape, a.dtype) for a in like]
         + [pltpu.SemaphoreType.DMA((8,)), pltpu.SemaphoreType.DMA((2, BLOCKS))],
         compiler_params=pltpu.CompilerParams(vmem_limit_bytes=20 * 1024 * 1024),
-    )(kfac, vfac, kw, vw, kf, ks, vf, vs, wall, total, squares)
+    )(*held, wall, total, squares)
 
 
 def solution(mesh):

time: 95.7 us -> 74 us (0.77)
  local copies, waits for them, and re-layouts: 13.1 us -> 0 us
  Pallas kernels: 81.4 us -> 73.1 us
    unnamed x22 -> x0, local copies, waits for them, and re-layouts: 13.1 us -> none
    pallas_call x1, Pallas kernels: 76.9 us -> 68.4 us  [exchange(): pl.pallas_call(functools.partial(kernel, plan), out_shape=out_shape, in_s...]
where the time goes in v3:
time: 74 us; the launch traced here: 73.8 us
  Pallas kernels  73.1 us (99%)
    pallas_call x1, Pallas kernels, exchange(): pl.pallas_call(functools.partial(kernel, plan), out_shape=out_shape, in_s...  68.4 us
    pallas_call x1, Pallas kernels, body(): pl.pallas_call(functools.partial(finish, plan), out_shape=like, in_specs=...  4.71 us

profile of v3, /device:TPU:0, one launch (start us, length us, event | category | flops | bytes accessed | tf_op | source)
XLA Modules:
  0.0 73.8 jit_solution(17290674859269352108)
XLA Ops:
  0.6 68.4 %shard_map.186 = (bf16[4,2,384,768]{3,2,1,0:T(8,128)(2,1)S(1)}, bf16[256,768]{1,0:T(8,128)(2,1)S(1)}, f32[8,128]{1,0:T(8,128)S(1)}, bf16[3072,256]{1,0:T(8,128)(...) custom-call(bf16[640,3072]{1,0:T(8,128)(2,1)} %x_hbm.1, ...), custom_call_target="tpu_custom_call" | custom-call | tf_op jit(solution)/shard_map/pallas_call | solution.py:372
  69.1 4.7 %shard_map.187 = (f32[384,256]{1,0:T(8,128)}, f32[384,512]{1,0:T(8,128)}, f32[256,256]{1,0:T(8,128)}, f32[256,256]{1,0:T(8,128)}, f32[256,512]{1,0:T(8,128)}, /*...) custom-call(bf16[3072,256]{1,0:T(8,128)(2,1)S(1)} %get-tuple-element, ...), custom_call_target="tpu_custom_call" | custom-call | tf_op jit(solution)/shard_map/pallas_call | solution.py:455

commit v4 on v3

--- a/solution.py
+++ b/solution.py
@@ -253,6 +253,7 @@
 
     relay(1, NH, NP)
 
+    relay(2, 0, NH)
     for j in range(1, F):
         src = lax.rem(z + F - j, F)
 
@@ -268,7 +269,8 @@
     for j in range(1, R):
         half_copy(j).start()
 
-    for s in range(2, F):
+    relay(2, NH, NP)
+    for s in range(3, F):
         relay(s, 0, NP)
 
     for j in range(1, R):

time: 74 us -> 71.6 us (0.968)
  Pallas kernels: 73.1 us -> 70.8 us
    pallas_call x1, Pallas kernels: 68.4 us -> 66.1 us  [exchange(): pl.pallas_call(functools.partial(kernel, plan), out_shape=out_shape, in_s...]
where the time goes in v4:
time: 71.6 us; the launch traced here: 71.4 us
  Pallas kernels  70.8 us (99%)
    pallas_call x1, Pallas kernels, exchange(): pl.pallas_call(functools.partial(kernel, plan), out_shape=out_shape, in_s...  66.1 us
    pallas_call x1, Pallas kernels, body(): pl.pallas_call(functools.partial(finish, plan), out_shape=like, in_specs=...  4.7 us

profile of v4, /device:TPU:0, one launch (start us, length us, event | category | flops | bytes accessed | tf_op | source)
XLA Modules:
  0.0 71.4 jit_solution(4612588708823694906)
XLA Ops:
  0.6 66.1 %shard_map.186 = (bf16[4,2,384,768]{3,2,1,0:T(8,128)(2,1)S(1)}, bf16[256,768]{1,0:T(8,128)(2,1)S(1)}, f32[8,128]{1,0:T(8,128)S(1)}, bf16[3072,256]{1,0:T(8,128)(...) custom-call(bf16[640,3072]{1,0:T(8,128)(2,1)} %x_hbm.1, ...), custom_call_target="tpu_custom_call" | custom-call | tf_op jit(solution)/shard_map/pallas_call | solution.py:374
  66.7 4.7 %shard_map.187 = (f32[384,256]{1,0:T(8,128)}, f32[384,512]{1,0:T(8,128)}, f32[256,256]{1,0:T(8,128)}, f32[256,256]{1,0:T(8,128)}, f32[256,512]{1,0:T(8,128)}, /*...) custom-call(bf16[3072,256]{1,0:T(8,128)(2,1)S(1)} %get-tuple-element, ...), custom_call_target="tpu_custom_call" | custom-call | tf_op jit(solution)/shard_map/pallas_call | solution.py:457
